TPU v7x, 32 devices: a whole 2x2x4 slice. The times are simulated.
32 devices in a mesh: kv: 16 (over z, y, x), tp: 2 (over core).
Axes of the slice: x: 2, y: 2, z: 4, core: 2. Of those that a mesh axis runs over, the one named last changes fastest.
Arguments:
- queries: bfloat16 [14336, 1024], P('kv', 'tp'), may hold values from -6 to 6
- keyvals: bfloat16 [14336, 128], P('kv'), may hold values from -6 to 6
- log_sums: float32 [16, 14336], P('tp', 'kv'), may hold values from 6 to 7.2
- out_grad: bfloat16 [14336, 1024], P('kv', 'tp'), may hold values from -24 to 24
- inputs: bfloat16 [14336, 2048], P('kv'), may hold values from -0.119628906 to 0.119628906
- selection: int32 [112, 16], replicated, may hold values from -1 to 447, as said below
Outputs:
- query_grad: bfloat16 [14336, 1024], P('kv', 'tp')
- keyval_grad: float32 [448, 32, 128], P('kv', 'tp')
- weight_grad: float32 [2048, 1024], P('kv', 'tp')
Inputs may be any that keep to these rules, and one draw needn't show every extreme that they name: `selection`: row j first names the key blocks of query block j's own positions in order, then distinct blocks of earlier devices' positions, then -1 entries at the end (only where fewer earlier blocks exist). The rows of one device's query blocks together name at most 2 distinct blocks of any one other device, and exactly 2 for some pair in every draw.
All inputs are finite; a program needn't handle non-finite values.
Results may differ from a plain program's by a relative error of at most 0.0071.
Values may be sent and summed in bfloat16 or wider, within the bound.
A program may use at most 64 MiB of HBM per device.

v0:
```python
import functools

import jax
import jax.numpy as jnp
from jax import lax
from jax.experimental import pallas as pl
from jax.experimental.pallas import tpu as pltpu
from jax.sharding import PartitionSpec as P

DH = 64
QB = 128
KB = 32
NSEL = 16
CAP = 2
LOG2E = 1.4426950408889634
DEAD = 1e30
GROUP = 1
UNROLL = True
MESH = pl.DeviceIdType.MESH


def slot_table(wanted):
    slot_rank = jnp.cumsum(wanted.astype(jnp.int32), axis=1) - 1
    return wanted[:, None, :] & (
        slot_rank[:, None, :] == jnp.arange(CAP, dtype=jnp.int32)[None, :, None]
    )


def weight_term(inputs, query_grad):
    return lax.dot_general(
        inputs, query_grad, (((0,), (0,)), ((), ())), preferred_element_type=jnp.float32
    )


def body(queries, keyvals, log_sums, out_grad, inputs, selection):
    kv_count = lax.axis_size("kv")
    own_index = lax.axis_index("kv")
    tok_count, width = queries.shape
    head_count = width // DH
    per_dev = tok_count // QB
    own_blocks = tok_count // KB
    slot_count = kv_count * CAP
    score_scale = DH ** (-0.5)
    own_kv = keyvals.reshape(own_blocks, KB, 2 * DH)
    lists = selection.reshape(kv_count, per_dev * NSEL)
    device_ids = jnp.arange(kv_count, dtype=jnp.int32)
    mine = own_index * own_blocks + jnp.arange(own_blocks, dtype=jnp.int32)
    wanted = jnp.any(lists[:, :, None] == mine[None, None, :], axis=1) & (
        device_ids[:, None] != own_index
    )
    owner_slots = slot_table(wanted)
    outgoing = jnp.einsum(
        "rsb,bkc->rskc",
        owner_slots.astype(jnp.bfloat16),
        own_kv,
        preferred_element_type=jnp.float32,
    ).astype(jnp.bfloat16)
    fetched = lax.all_to_all(outgoing, "kv", split_axis=0, concat_axis=0, tiled=True)
    block_list = lax.dynamic_index_in_dim(lists, own_index, 0, keepdims=False)
    every_block = jnp.arange(kv_count * own_blocks, dtype=jnp.int32)
    hits = block_list[:, None] == every_block[None, :]
    needed = jnp.any(hits, axis=0).reshape(kv_count, own_blocks) & (
        device_ids[:, None] != own_index
    )
    slot_rank = jnp.cumsum(needed.astype(jnp.int32), axis=1) - 1
    entry_rank = jnp.sum(jnp.where(hits, slot_rank.reshape(-1)[None, :], 0), axis=1)
    safe_list = jnp.maximum(block_list, 0)
    owner_index = safe_list // own_blocks
    local_block = safe_list % own_blocks
    pool_index = jnp.where(
        owner_index == own_index, slot_count + local_block, owner_index * CAP + entry_rank
    )
    pool_index = jnp.where(block_list < 0, 0, pool_index)
    block_pool = jnp.concatenate([fetched.reshape(slot_count, KB, 2 * DH), own_kv], axis=0)
    gathered = jnp.take(block_pool, pool_index, axis=0).reshape(per_dev, NSEL * KB, 2 * DH)
    key_rows = gathered[:, :, :DH]
    value_rows = gathered[:, :, DH:]
    query_rows = queries.reshape(per_dev, QB, head_count, DH)
    grad_rows = out_grad.reshape(per_dev, QB, head_count, DH)
    log_rows = log_sums.reshape(head_count, per_dev, QB).transpose(1, 0, 2)
    key_pos = (
        safe_list.reshape(per_dev, NSEL, 1) * KB + jnp.arange(KB, dtype=jnp.int32)[None, None, :]
    ).reshape(per_dev, NSEL * KB)
    key_live = jnp.repeat((block_list >= 0).reshape(per_dev, NSEL), KB, axis=1)
    query_pos = own_index * tok_count + jnp.arange(tok_count, dtype=jnp.int32).reshape(per_dev, QB)
    live_mask = key_live[:, None, :] & (key_pos[:, None, :] <= query_pos[:, :, None])
    scores = (
        jnp.einsum("pthd,pkd->phtk", query_rows, key_rows, preferred_element_type=jnp.float32)
        * score_scale
    )
    prob_f32 = jnp.where(live_mask[:, None], jnp.exp(scores - log_rows[..., None]), 0.0)
    prob_b = prob_f32.astype(jnp.bfloat16)
    recomputed = jnp.einsum(
        "phtk,pkd->pthd", prob_b, value_rows, preferred_element_type=jnp.float32
    )
    row_delta = jnp.sum(grad_rows.astype(jnp.float32) * recomputed, axis=-1)
    dprob = jnp.einsum("pthd,pkd->phtk", grad_rows, value_rows, preferred_element_type=jnp.float32)
    dscore = prob_f32 * (dprob - row_delta.transpose(0, 2, 1)[..., None])
    dscore_b = dscore.astype(jnp.bfloat16)
    query_grad = (
        (
            jnp.einsum("phtk,pkd->pthd", dscore_b, key_rows, preferred_element_type=jnp.float32)
            * score_scale
        )
        .astype(jnp.bfloat16)
        .reshape(tok_count, width)
    )
    key_grad = (
        jnp.einsum("phtk,pthd->pkd", dscore_b, query_rows, preferred_element_type=jnp.float32)
        * score_scale
    )
    value_grad = jnp.einsum("phtk,pthd->pkd", prob_b, grad_rows, preferred_element_type=jnp.float32)
    entry_grads = jnp.concatenate([key_grad, value_grad], axis=-1).reshape(
        per_dev * NSEL, KB, 2 * DH
    )
    spread = (
        pool_index[:, None] == jnp.arange(slot_count + own_blocks, dtype=jnp.int32)[None, :]
    ).astype(jnp.float32)
    shares = lax.psum_scatter(entry_grads, "tp", scatter_dimension=1, tiled=True)
    summed = jnp.einsum("ep,ekc->pkc", spread, shares, precision=lax.Precision.HIGHEST)
    key_share = summed.shape[1]
    returned = lax.all_to_all(
        summed[:slot_count].reshape(kv_count, CAP, key_share, 2 * DH).astype(jnp.bfloat16),
        "kv",
        split_axis=0,
        concat_axis=0,
        tiled=True,
    ).astype(jnp.float32)
    keyval_grad = (
        jnp.einsum(
            "rsb,rskc->bkc",
            owner_slots.astype(jnp.float32),
            returned,
            precision=lax.Precision.HIGHEST,
        )
        + summed[slot_count:]
    )
    weight_grad = lax.psum_scatter(
        weight_term(inputs, query_grad), "kv", scatter_dimension=0, tiled=True
    )
    return (query_grad, keyval_grad, weight_grad)


def bit_orders(kv_count, chunk_count):
    bits = kv_count.bit_length() - 1
    orders = []
    for c in range(chunk_count):
        turn = c % 3
        first = [0, 1, 2]
        orders.append(first[turn:] + first[:turn] + list(range(3, bits)))
    return orders


def flip(index, place):
    bit = (index // (1 << place)) % 2
    return index + (1 - 2 * bit) * (1 << place)


def fused_kernel(
    kv_count,
    orders,
    index_ref,
    list_ref,
    place_ref,
    out_ref,
    own_kv_ref,
    log_ref,
    q_hbm,
    g_hbm,
    in_hbm,
    qg_ref,
    wg_ref,
    own_ref,
    ret_ref,
    q_scr,
    g_scr,
    in_scr,
    pool_scr,
    kv_scr,
    kt_scr,
    dkv_scr,
    qgt_scr,
    total,
    half_scr,
    tp_scr,
    slot_scr,
    ret_scr,
    *rest,
):
    bits = len(orders[0])
    chunk_count = len(orders)
    send_scr = rest[:bits]
    recv_scr = rest[bits : 2 * bits]
    load_sem, get_send, get_recv, tp_send, tp_recv, ret_send, ret_recv, w_send, w_recv = rest[2 * bits :]
    me = lax.axis_index("kv")
    core = lax.axis_index("tp")
    other = 1 - core
    rows, width = wg_ref.shape
    pair_count = width // (2 * DH * GROUP)
    per_dev = q_scr.shape[0] // QB
    slot_count = kv_count * CAP
    entry_count = per_dev * NSEL
    diagonal = QB // KB
    half = KB // 2
    score_scale = DH ** (-0.5)

    def peer(step):
        return lax.rem(me + step, kv_count)

    loads = [
        pltpu.make_async_copy(src, dst, load_sem.at[i])
        for i, (src, dst) in enumerate(((q_hbm, q_scr), (g_hbm, g_scr), (in_hbm, in_scr)))
    ]
    for load in loads:
        load.start()

    barrier = pltpu.get_barrier_semaphore()
    for step in range(1, kv_count):
        pl.semaphore_signal(barrier, inc=1, device_id=(peer(step), core), device_id_type=MESH)
    pl.semaphore_signal(barrier, inc=1, device_id=(me, other), device_id_type=MESH)
    pl.semaphore_wait(barrier, kv_count)

    def get_copy(target, source):
        return pltpu.make_async_remote_copy(
            src_ref=out_ref.at[target],
            dst_ref=pool_scr.at[pl.ds(source * CAP, CAP)],
            send_sem=get_send.at[target],
            recv_sem=get_recv.at[source],
            device_id=(target, core),
            device_id_type=MESH,
        )

    for step in range(1, kv_count):
        get_copy(peer(step), me).start()
    pool_scr[pl.ds(me * CAP, CAP)] = jnp.zeros((CAP, KB, 2 * DH), jnp.bfloat16)
    pool_scr[slot_count:] = own_kv_ref[...]
    dkv_scr[entry_count] = jnp.zeros((KB, 2 * DH), jnp.float32)
    for load in loads[:2]:
        load.wait()
    for step in range(1, kv_count):
        get_copy(me, peer(step)).wait_recv()

    def gather(p, carry):
        for e in range(NSEL):
            kv_scr[p, e * KB : (e + 1) * KB, :] = pool_scr[index_ref[p * NSEL + e]]
        kt_scr[p] = kv_scr[p][:, :DH].T
        return carry

    lax.fori_loop(0, per_dev, gather, 0)

    key_row = lax.broadcasted_iota(jnp.int32, (QB, 2 * QB), 0)
    query_col = lax.broadcasted_iota(jnp.int32, (QB, 2 * QB), 1) % QB
    causal = key_row <= query_col
    nt = (((1,), (1,)), ((), ()))

    def attend(group):
        def block(p, carry):
            tok = pl.ds(pl.multiple_of(p * QB, QB), QB)
            keys = kv_scr[p, :, :DH]
            values = kv_scr[p, :, DH:]
            penalty = [
                jnp.where(list_ref[p * NSEL + e] >= 0, jnp.float32(0.0), jnp.float32(DEAD))
                for e in range(NSEL)
            ]
            dkv = None
            for pair in range(group * GROUP, (group + 1) * GROUP):
                at = pair * 2 * DH
                q2 = jnp.concatenate([q_scr[tok, at : at + DH], q_scr[tok, at + DH : at + 2 * DH]], axis=0)
                g2 = jnp.concatenate([g_scr[tok, at : at + DH], g_scr[tok, at + DH : at + 2 * DH]], axis=0)
                log2 = jnp.concatenate(
                    [log_ref[2 * pair : 2 * pair + 1, tok], log_ref[2 * pair + 1 : 2 * pair + 2, tok]], axis=1
                )
                log2 = log2 * LOG2E
                scores = lax.dot_general(keys, q2, nt, preferred_element_type=jnp.float32)
                dprob = lax.dot_general(values, g2, nt, preferred_element_type=jnp.float32)
                shifted = jnp.concatenate(
                    [
                        scores[e * KB : (e + 1) * KB] * (score_scale * LOG2E) - (log2 + penalty[e])
                        for e in range(NSEL)
                    ],
                    axis=0,
                )
                shifted = jnp.concatenate([jnp.where(causal, shifted[:QB], -DEAD), shifted[QB:]], axis=0)
                prob = jnp.exp2(shifted)
                prob_b = prob.astype(jnp.bfloat16)
                delta = jnp.sum(prob_b.astype(jnp.float32) * dprob, axis=0, keepdims=True)
                dscore_b = (prob * (dprob - delta)).astype(jnp.bfloat16)
                dq = jnp.dot(kt_scr[p], dscore_b, preferred_element_type=jnp.float32) * score_scale
                dq = jnp.concatenate([dq[:, :QB], dq[:, QB:]], axis=0)
                qgt_scr[at : at + 2 * DH, tok] = dq.astype(jnp.bfloat16)
                qg_ref[tok, at : at + 2 * DH] = dq.T.astype(jnp.bfloat16)
                dk = jnp.dot(dscore_b, q2, preferred_element_type=jnp.float32) * score_scale
                dv = jnp.dot(prob_b, g2, preferred_element_type=jnp.float32)
                part = jnp.concatenate([dk, dv], axis=1)
                dkv = part if dkv is None else dkv + part
            dkv = dkv.reshape(NSEL, KB, 2 * DH)
            entries = pl.ds(p * NSEL, NSEL)
            if group > 0:
                dkv = dkv + dkv_scr[entries]
            dkv_scr[entries] = dkv
            return carry

        lax.fori_loop(0, per_dev, block, 0, unroll=UNROLL)

    def product(pair):
        cols = slice(pair * GROUP * 2 * DH, (pair + 1) * GROUP * 2 * DH)

        def piece(j, carry):
            at = pl.multiple_of(j * 2 * rows, 2 * rows)
            part = jnp.dot(
                qgt_scr[cols, :], in_scr[:, pl.ds(at, 2 * rows)], preferred_element_type=jnp.float32
            )
            total[2 * j, cols, :] = part[:, :rows]
            total[2 * j + 1, cols, :] = part[:, rows:]
            return carry

        lax.fori_loop(0, kv_count // 2, piece, 0)

    def owner_of(c, slot):
        owner = me
        for k in range(bits):
            if (slot >> (bits - 1 - k)) & 1:
                owner = flip(owner, orders[c][k])
        return owner

    def current(c, slot, k):
        at = owner_of(c, slot)
        value = total[at, c * DH : (c + 1) * DH, :]
        if k > 0:
            value = value + recv_scr[k - 1][c, slot].astype(jnp.float32)
            total[at, c * DH : (c + 1) * DH, :] = value
        return value

    def weight_copy(c, k):
        return pltpu.make_async_remote_copy(
            src_ref=send_scr[k].at[c],
            dst_ref=recv_scr[k].at[c],
            send_sem=w_send.at[c, k],
            recv_sem=w_recv.at[c, k],
            device_id=(flip(me, orders[c][k]), core),
            device_id_type=MESH,
        )

    def weight_stage(pair, k):
        left = kv_count >> (k + 1)
        for c in range(2 * GROUP * pair, 2 * GROUP * (pair + 1)):
            if k > 0:
                weight_copy(c, k - 1).wait_recv()
            if k == bits:
                value = total[me, c * DH : (c + 1) * DH, :] + recv_scr[k - 1][c, 0].astype(jnp.float32)
                wg_ref[:, c * DH : (c + 1) * DH] = value.T
                continue
            for slot in range(left, 2 * left):
                send_scr[k][c, slot - left] = current(c, slot, k).astype(jnp.bfloat16)
            weight_copy(c, k).start()
            if k > 0:
                for slot in range(left):
                    current(c, slot, k)

    def advance(turn):
        for k in range(bits + 1):
            if 0 <= turn - k < pair_count:
                weight_stage(turn - k, k)

    tp_copy = pltpu.make_async_remote_copy(
        src_ref=half_scr.at[other],
        dst_ref=tp_scr,
        send_sem=tp_send,
        recv_sem=tp_recv,
        device_id=(me, other),
        device_id_type=MESH,
    )

    def ret_copy(target, source):
        return pltpu.make_async_remote_copy(
            src_ref=slot_scr.at[target],
            dst_ref=ret_scr.at[source],
            send_sem=ret_send.at[target],
            recv_sem=ret_recv.at[source],
            device_id=(target, core),
            device_id_type=MESH,
        )

    def collect(s, carry):
        value = dkv_scr[place_ref[s * per_dev]]
        for p in range(1, per_dev):
            value = value + dkv_scr[place_ref[s * per_dev + p]]
        half_scr[0, s] = value[:half]
        half_scr[1, s] = value[half:]
        return carry

    for pair in range(pair_count):
        attend(pair)
        if pair == 0:
            loads[2].wait()
        if pair == pair_count - 1:
            lax.fori_loop(0, slot_count, collect, 0)
            for p in range(per_dev):
                at = slot_count + p * diagonal
                half_scr[0, at : at + diagonal] = dkv_scr[p * NSEL : p * NSEL + diagonal, :half, :]
                half_scr[1, at : at + diagonal] = dkv_scr[p * NSEL : p * NSEL + diagonal, half:, :]
            tp_copy.start()
        product(pair)
        advance(pair)

    tp_copy.wait_recv()
    mine = half_scr.at[core]
    slot_scr[...] = (
        (mine[:slot_count] + tp_scr[:slot_count])
        .astype(jnp.bfloat16)
        .reshape(kv_count, CAP, half, 2 * DH)
    )
    ret_scr[me] = jnp.zeros(ret_scr.shape[1:], jnp.bfloat16)
    for step in range(1, kv_count):
        ret_copy(peer(step), me).start()
    own_ref[...] = mine[slot_count:] + tp_scr[slot_count:]

    for turn in range(pair_count, pair_count + bits):
        advance(turn)
    for step in range(1, kv_count):
        ret_copy(me, peer(step)).wait_recv()
    ret_ref[...] = ret_scr[...]
    for step in range(1, kv_count):
        get_copy(peer(step), me).wait_send()
        ret_copy(peer(step), me).wait_send()
    tp_copy.wait_send()
    for c in range(chunk_count):
        for k in range(bits):
            weight_copy(c, k).wait_send()


def fused(kv_count, pool_index, block_list, place, outgoing, own_kv, log_sums, queries, out_grad, inputs):
    tok_count, width = queries.shape
    per_dev = tok_count // QB
    rows = inputs.shape[1] // kv_count
    chunk_count = width // DH
    orders = bit_orders(kv_count, chunk_count)
    bits = len(orders[0])
    slot_count = kv_count * CAP
    pool_count = slot_count + own_kv.shape[0]
    half = KB // 2
    parts = [
        pltpu.VMEM((chunk_count, kv_count >> (k + 1), DH, rows), jnp.bfloat16) for k in range(bits)
    ]
    vmem = pl.BlockSpec(memory_space=pltpu.VMEM)
    smem = pl.BlockSpec(memory_space=pltpu.SMEM)
    hbm = pl.BlockSpec(memory_space=pl.ANY)
    dma = pltpu.SemaphoreType.DMA
    return pl.pallas_call(
        functools.partial(fused_kernel, kv_count, orders),
        out_shape=[
            jax.ShapeDtypeStruct((tok_count, width), jnp.bfloat16),
            jax.ShapeDtypeStruct((rows, width), jnp.float32),
            jax.ShapeDtypeStruct((own_kv.shape[0], half, 2 * DH), jnp.float32),
            jax.ShapeDtypeStruct((kv_count, CAP, half, 2 * DH), jnp.bfloat16),
        ],
        in_specs=[smem] * 3 + [vmem] * 3 + [hbm] * 3,
        out_specs=[vmem] * 4,
        scratch_shapes=[
            pltpu.VMEM((tok_count, width), jnp.bfloat16),
            pltpu.VMEM((tok_count, width), jnp.bfloat16),
            pltpu.VMEM(inputs.shape, jnp.bfloat16),
            pltpu.VMEM((pool_count, KB, 2 * DH), jnp.bfloat16),
            pltpu.VMEM((per_dev, NSEL * KB, 2 * DH), jnp.bfloat16),
            pltpu.VMEM((per_dev, DH, NSEL * KB), jnp.bfloat16),
            pltpu.VMEM((per_dev * NSEL + 1, KB, 2 * DH), jnp.float32),
            pltpu.VMEM((width, tok_count), jnp.bfloat16),
            pltpu.VMEM((kv_count, width, rows), jnp.float32),
            pltpu.VMEM((2, pool_count, half, 2 * DH), jnp.float32),
            pltpu.VMEM((pool_count, half, 2 * DH), jnp.float32),
            pltpu.VMEM((kv_count, CAP, half, 2 * DH), jnp.bfloat16),
            pltpu.VMEM((kv_count, CAP, half, 2 * DH), jnp.bfloat16),
        ]
        + parts
        + parts
        + [
            dma((3,)),
            dma((kv_count,)),
            dma((kv_count,)),
            dma,
            dma,
            dma((kv_count,)),
            dma((kv_count,)),
            dma((chunk_count, bits)),
            dma((chunk_count, bits)),
        ],
        compiler_params=pltpu.CompilerParams(
            collective_id=0, has_side_effects=True, vmem_limit_bytes=60 * 1024 * 1024
        ),
        name="fused",
    )(pool_index, block_list, place, outgoing, own_kv, log_sums, queries, out_grad, inputs)


def fused_body(queries, keyvals, log_sums, out_grad, inputs, selection):
    kv_count = lax.axis_size("kv")
    own_index = lax.axis_index("kv")
    tok_count, width = queries.shape
    per_dev = tok_count // QB
    own_blocks = tok_count // KB
    slot_count = kv_count * CAP
    own_kv = keyvals.reshape(own_blocks, KB, 2 * DH)
    lists = selection.reshape(kv_count, per_dev * NSEL)
    device_ids = jnp.arange(kv_count, dtype=jnp.int32)
    mine = own_index * own_blocks + jnp.arange(own_blocks, dtype=jnp.int32)
    wanted = jnp.any(lists[:, :, None] == mine[None, None, :], axis=1) & (
        device_ids[:, None] != own_index
    )
    owner_slots = slot_table(wanted)
    outgoing = jnp.einsum(
        "rsb,bkc->rskc",
        owner_slots.astype(jnp.bfloat16),
        own_kv,
        preferred_element_type=jnp.float32,
    ).astype(jnp.bfloat16)
    block_list = lax.dynamic_index_in_dim(lists, own_index, 0, keepdims=False)
    every_block = jnp.arange(kv_count * own_blocks, dtype=jnp.int32)
    hits = block_list[:, None] == every_block[None, :]
    needed = jnp.any(hits, axis=0).reshape(kv_count, own_blocks) & (
        device_ids[:, None] != own_index
    )
    slot_rank = jnp.cumsum(needed.astype(jnp.int32), axis=1) - 1
    entry_rank = jnp.sum(jnp.where(hits, slot_rank.reshape(-1)[None, :], 0), axis=1)
    safe_list = jnp.maximum(block_list, 0)
    owner_index = safe_list // own_blocks
    local_block = safe_list % own_blocks
    pool_index = jnp.where(
        owner_index == own_index, slot_count + local_block, owner_index * CAP + entry_rank
    )
    pool_index = jnp.where(block_list < 0, slot_count, pool_index)
    entry_ids = jnp.arange(per_dev * NSEL, dtype=jnp.int32).reshape(1, per_dev, NSEL)
    slot_ids = jnp.arange(slot_count, dtype=jnp.int32)[:, None, None]
    spare = per_dev * NSEL
    place = spare + jnp.sum(
        jnp.where(pool_index.reshape(1, per_dev, NSEL) == slot_ids, entry_ids - spare, 0), axis=2
    )
    query_grad, weight_grad, own_grad, returned = fused(
        kv_count,
        pool_index,
        block_list,
        place.reshape(-1),
        outgoing,
        own_kv,
        log_sums,
        queries,
        out_grad,
        inputs,
    )
    keyval_grad = own_grad + jnp.einsum(
        "rsb,rskc->bkc",
        owner_slots.astype(jnp.bfloat16),
        returned,
        preferred_element_type=jnp.float32,
    )
    return (query_grad, keyval_grad, weight_grad)


def fits(kv_count, tp_count, rows, width):
    power = kv_count & (kv_count - 1) == 0 and kv_count >= 8
    return tp_count == 2 and power and rows % 128 == 0 and width % (2 * DH * GROUP) == 0


def step(queries, keyvals, log_sums, out_grad, inputs, selection):
    kv_count, tp_count = lax.axis_size("kv"), lax.axis_size("tp")
    chosen = fits(kv_count, tp_count, inputs.shape[1] // kv_count, queries.shape[1])
    return (fused_body if chosen else body)(
        queries, keyvals, log_sums, out_grad, inputs, selection
    )


def solution(mesh):
    return jax.shard_map(
        step,
        mesh=mesh,
        in_specs=(P("kv", "tp"), P("kv", None), P("tp", "kv"), P("kv", "tp"), P("kv", None), P()),
        out_specs=(P("kv", "tp"), P("kv", "tp", None), P("kv", "tp")),
        check_vma=False,
    )
```

profile of v0, /device:TPU:0, one launch (start us, length us, event | category | flops | bytes accessed | tf_op | source)
XLA Modules:
  0.0 74.0 jit_solution(4016887170837854555)
XLA Ops:
  0.6 0.8 %copy.37 = s32[112,16]{1,0:T(8,128)S(1)} copy(s32[112,16]{0,1:T(8,128)} %param.11) | data formatting | bytes 14336 | tf_op args[5]
  1.4 0.1 reshape.133
  1.5 0.0 copy-start
  1.6 0.1 fusion.3
  1.7 0.1 reshape.134
  1.8 0.6 compare_reduce_fusion
  2.4 0.1 copy.39
  2.5 0.1 fusion.18
  2.6 0.2 reduce_window_sum.18
  2.8 1.2 %fusion = bf16[16,2,32,128]{3,0,2,1:T(8,128)(2,1)S(1)} fusion(bf16[28,32,128]{2,1,0:T(8,128)(2,1)} %bitcast.16, s32[16,28]{1,0:T(8,128)S(1)} %broadcast_add_fusion, pred[16,28]{1,0:T(8,128)(4,1)S(1)} %get-tuple-element.16), kind=kOutput, calls=%fused_computation.2 | convolution fusion | flops 7341824 | bytes 493760 | tf_op jit(solution)/shard_map/rsb,bkc->rskc/dot_general | solution.py:509
  3.9 0.8 %copy.54.out_ref = bf16[16,2,32,128]{3,2,1,0:T(8,128)(2,1)} copy(bf16[16,2,32,128]{3,0,2,1:T(8,128)(2,1)S(1)} %fusion) | data formatting | bytes 524288 | tf_op jit(solution)/shard_map/rsb,bkc->rskc/dot_general | solution.py:509
  4.7 0.2 reduce_window_sum.17
  4.9 0.1 sub.22
  5.0 0.2 select_reduce_fusion
  5.2 0.1 reduce_sum.21
  5.3 0.1 lt.28
  5.4 0.1 ne.62
  5.5 0.1 div.17
  5.5 0.1 rem.30
  5.6 0.1 select_reduce_fusion.1
  5.8 0.1 copy.38
  5.9 0.7 add.95.place_ref
  6.5 0.5 compare_select_fusion.1.index_ref
  7.1 0.0 copy-done
  7.1 60.2 %fused.1 = (bf16[896,512]{1,0:T(8,128)(2,1)}, f32[128,512]{1,0:T(8,128)}, f32[28,16,128]{2,1,0:T(8,128)}, bf16[16,2,16,128]{3,2,1,0:T(8,128)(2,1)}) custom-call(s32[112]{0:T(128)} %compare_select_fusion.1.index_ref, s32[112]{0:T(128)} %bitcast.20, s32[224]{0:T(256)} %add.95.place_ref, bf16[16,2,32,128]{3,2,1,0:T(8,128)(2,1)} %copy.54.out_ref, ...), custom_call_target="tpu_custom_call" | custom-call | tf_op jit(solution)/shard_map/fused/pallas_call | solution.py:449
  67.3 1.1 %convolution_bitcast_fusion = f32[28,16,128]{2,0,1:T(8,128)S(1)} fusion(bf16[16,2,16,128]{3,2,1,0:T(8,128)(2,1)} %get-tuple-element.9, s32[16,28]{1,0:T(8,128)S(1)} %broadcast_add_fusion, pred[16,28]{1,0:T(8,128)(4,1)S(1)} %get-tuple-element.16), kind=kOutput, calls=%fused_computation | convolution fusion | flops 3671808 | bytes 362688 | tf_op jit(solution)/shard_map/rsb,rskc->bkc/dot_general | solution.py:548
  68.4 1.8 %copy_add_fusion = f32[28,16,128]{2,1,0:T(8,128)} fusion(f32[28,16,128]{2,1,0:T(8,128)} %get-tuple-element.8, f32[28,16,128]{2,0,1:T(8,128)S(1)} %convolution_bitcast_fusion), kind=kLoop, calls=%fused_computation.5 | loop fusion | flops 57344 | bytes 688128 | tf_op jit(solution)/shard_map/add | solution.py:548
  70.2 2.2 %copy.57 = bf16[896,512]{1,0:T(8,128)(2,1)} copy(bf16[896,512]{1,0:T(8,128)(2,1)} %get-tuple-element.24) | data formatting | bytes 1835008
  72.3 1.7 %copy.58 = f32[128,512]{1,0:T(8,128)} copy(f32[128,512]{1,0:T(8,128)} %get-tuple-element.26) | data formatting | bytes 524288
  (8 shorter events, 0.1 us)
Async XLA Ops:
  1.5 5.5 %copy-start = (s32[1,112]{1,0:T(1,128)}, s32[1,112]{1,0:T(1,128)S(1)}, u32[]{:S(2)}) copy-start(s32[1,112]{1,0:T(1,128)S(1)} %get-tuple-element.17) | copy-start | bytes 1348
where the time goes:
time: 74.3 us; the launch traced here: 74 us
  Pallas kernels  60.2 us (81%)
  local copies, waits for them, and re-layouts  6.91 us (9%)
  other arithmetic  3.88 us (5%)
  matrix products  2.29 us (3%)
    pallas_call x1, Pallas kernels, fused(): pl.pallas_call(functools.partial(fused_kernel, kv_count, orders), out_sha...  60.2 us
    unnamed x5, local copies, waits for them, and re-layouts  4.63 us
    add x1, other arithmetic, fused_body(): own_grad + jnp.einsum('rsb,rskc->bkc', owner_slots.astype(jnp.bfloat16),...  1.77 us

commit v1 on v0

--- a/solution.py
+++ b/solution.py
@@ -16,6 +16,7 @@
 DEAD = 1e30
 GROUP = 1
 UNROLL = True
+VMEM_LIMIT = 28 * 1024 * 1024
 MESH = pl.DeviceIdType.MESH
 
 
@@ -159,19 +160,23 @@
 def fused_kernel(
     kv_count,
     orders,
-    index_ref,
-    list_ref,
-    place_ref,
-    out_ref,
-    own_kv_ref,
-    log_ref,
+    sel_hbm,
+    own_hbm,
+    log_hbm,
     q_hbm,
     g_hbm,
     in_hbm,
     qg_ref,
     wg_ref,
-    own_ref,
-    ret_ref,
+    kvg_ref,
+    sel_scr,
+    first_scr,
+    table_scr,
+    first_ref,
+    table_ref,
+    out_scr,
+    log_ref,
+    own_scr,
     q_scr,
     g_scr,
     in_scr,
@@ -207,22 +212,49 @@
     def peer(step):
         return lax.rem(me + step, kv_count)
 
+    own_blocks = own_hbm.shape[0]
     loads = [
         pltpu.make_async_copy(src, dst, load_sem.at[i])
-        for i, (src, dst) in enumerate(((q_hbm, q_scr), (g_hbm, g_scr), (in_hbm, in_scr)))
+        for i, (src, dst) in enumerate(
+            (
+                (sel_hbm, sel_scr),
+                (own_hbm, own_scr),
+                (log_hbm, log_ref),
+                (q_hbm, q_scr),
+                (g_hbm, g_scr),
+                (in_hbm, in_scr),
+                (first_scr, first_ref),
+                (table_scr, table_ref),
+            )
+        )
     ]
-    for load in loads:
+    for load in loads[:6]:
         load.start()
+    pool_scr[...] = jnp.zeros(pool_scr.shape, jnp.bfloat16)
+    ret_scr[...] = jnp.zeros(ret_scr.shape, jnp.bfloat16)
 
     barrier = pltpu.get_barrier_semaphore()
     for step in range(1, kv_count):
         pl.semaphore_signal(barrier, inc=1, device_id=(peer(step), core), device_id_type=MESH)
     pl.semaphore_signal(barrier, inc=1, device_id=(me, other), device_id_type=MESH)
+
+    loads[0].wait()
+    chosen = padded(sel_scr[...])
+    first_scr[...] = first_table(chosen, me * own_blocks, own_blocks, per_dev)
+    loads[6].start()
+    table_scr[...] = entry_table(chosen, me, kv_count, own_blocks, per_dev)
+    loads[7].start()
+    dkv_scr[entry_count] = jnp.zeros((KB, 2 * DH), jnp.float32)
+    loads[1].wait()
+    loads[6].wait()
+    for r in range(kv_count):
+        for s in range(CAP):
+            out_scr[r, s] = own_scr[first_ref[s, r * per_dev]]
     pl.semaphore_wait(barrier, kv_count)
 
     def get_copy(target, source):
         return pltpu.make_async_remote_copy(
-            src_ref=out_ref.at[target],
+            src_ref=out_scr.at[target],
             dst_ref=pool_scr.at[pl.ds(source * CAP, CAP)],
             send_sem=get_send.at[target],
             recv_sem=get_recv.at[source],
@@ -230,19 +262,29 @@
             device_id_type=MESH,
         )
 
-    for step in range(1, kv_count):
-        get_copy(peer(step), me).start()
-    pool_scr[pl.ds(me * CAP, CAP)] = jnp.zeros((CAP, KB, 2 * DH), jnp.bfloat16)
-    pool_scr[slot_count:] = own_kv_ref[...]
-    dkv_scr[entry_count] = jnp.zeros((KB, 2 * DH), jnp.float32)
-    for load in loads[:2]:
+    def later(do):
+        for step in range(kv_count - 1, 0, -1):
+            @pl.when(me + step < kv_count)
+            def _():
+                do(me + step)
+
+    def earlier(do):
+        for step in range(1, kv_count):
+            @pl.when(me >= step)
+            def _():
+                do(me - step)
+
+    later(lambda r: get_copy(r, me).start())
+    for load in loads[2:5]:
         load.wait()
-    for step in range(1, kv_count):
-        get_copy(me, peer(step)).wait_recv()
+    loads[7].wait()
+    earlier(lambda r: get_copy(me, r).wait_recv())
 
     def gather(p, carry):
-        for e in range(NSEL):
-            kv_scr[p, e * KB : (e + 1) * KB, :] = pool_scr[index_ref[p * NSEL + e]]
+        for e in range(diagonal):
+            kv_scr[p, e * KB : (e + 1) * KB, :] = own_scr[p * diagonal + e]
+        for e in range(diagonal, NSEL):
+            kv_scr[p, e * KB : (e + 1) * KB, :] = pool_scr[table_ref[e, p]]
         kt_scr[p] = kv_scr[p][:, :DH].T
         return carry
 
@@ -259,7 +301,7 @@
             keys = kv_scr[p, :, :DH]
             values = kv_scr[p, :, DH:]
             penalty = [
-                jnp.where(list_ref[p * NSEL + e] >= 0, jnp.float32(0.0), jnp.float32(DEAD))
+                jnp.where(table_ref[NSEL + e, p] >= 0, jnp.float32(0.0), jnp.float32(DEAD))
                 for e in range(NSEL)
             ]
             dkv = None
@@ -382,9 +424,9 @@
         )
 
     def collect(s, carry):
-        value = dkv_scr[place_ref[s * per_dev]]
+        value = dkv_scr[table_ref[2 * NSEL + s, 0]]
         for p in range(1, per_dev):
-            value = value + dkv_scr[place_ref[s * per_dev + p]]
+            value = value + dkv_scr[table_ref[2 * NSEL + s, p]]
         half_scr[0, s] = value[:half]
         half_scr[1, s] = value[half:]
         return carry
@@ -392,7 +434,7 @@
     for pair in range(pair_count):
         attend(pair)
         if pair == 0:
-            loads[2].wait()
+            loads[5].wait()
         if pair == pair_count - 1:
             lax.fori_loop(0, slot_count, collect, 0)
             for p in range(per_dev):
@@ -410,26 +452,103 @@
         .astype(jnp.bfloat16)
         .reshape(kv_count, CAP, half, 2 * DH)
     )
-    ret_scr[me] = jnp.zeros(ret_scr.shape[1:], jnp.bfloat16)
-    for step in range(1, kv_count):
-        ret_copy(peer(step), me).start()
-    own_ref[...] = mine[slot_count:] + tp_scr[slot_count:]
+    earlier(lambda r: ret_copy(r, me).start())
+    own_sum = (mine[slot_count:] + tp_scr[slot_count:]).reshape(own_blocks * half, 2 * DH)
 
     for turn in range(pair_count, pair_count + bits):
         advance(turn)
-    for step in range(1, kv_count):
-        ret_copy(me, peer(step)).wait_recv()
-    ret_ref[...] = ret_scr[...]
-    for step in range(1, kv_count):
-        get_copy(peer(step), me).wait_send()
-        ret_copy(peer(step), me).wait_send()
+    later(lambda r: ret_copy(me, r).wait_recv())
+    column = lax.broadcasted_iota(jnp.int32, (1, slot_count * half), 1)
+    block = jnp.zeros(column.shape, jnp.int32)
+    for r in range(kv_count):
+        for s in range(CAP):
+            block = jnp.where(column // half == r * CAP + s, first_ref[s, r * per_dev], block)
+    wanted = block * half + column % half
+    row = lax.broadcasted_iota(jnp.int32, (own_blocks * half, slot_count * half), 0)
+    spread = jnp.where(row == wanted, 1.0, 0.0).astype(jnp.bfloat16)
+    back = ret_scr[...].reshape(slot_count * half, 2 * DH)
+    kvg = own_sum + jnp.dot(spread, back, preferred_element_type=jnp.float32)
+    kvg_ref[...] = kvg.reshape(own_blocks, half, 2 * DH)
+    later(lambda r: get_copy(r, me).wait_send())
+    earlier(lambda r: ret_copy(r, me).wait_send())
     tp_copy.wait_send()
     for c in range(chunk_count):
         for k in range(bits):
             weight_copy(c, k).wait_send()
 
 
-def fused(kv_count, pool_index, block_list, place, outgoing, own_kv, log_sums, queries, out_grad, inputs):
+def padded(chosen):
+    fill = jnp.full((NSEL, 128 - chosen.shape[1]), -1, jnp.int32)
+    return jnp.concatenate([chosen, fill], axis=1)
+
+
+def first_table(chosen, base, own_blocks, per_dev):
+    inside = (chosen >= base) & (chosen < base + own_blocks)
+    low = jnp.min(jnp.where(inside, chosen - base, own_blocks), axis=0, keepdims=True)
+    high = jnp.max(jnp.where(inside, chosen - base, -1), axis=0, keepdims=True)
+    cover = 1
+    while cover < per_dev:
+        shift = 128 - min(cover, per_dev - cover)
+        low = jnp.minimum(low, pltpu.roll(low, shift, 1))
+        high = jnp.maximum(high, pltpu.roll(high, shift, 1))
+        cover = min(2 * cover, per_dev)
+    low = jnp.where(low == own_blocks, 0, low)
+    high = jnp.maximum(high, 0)
+    row = lax.broadcasted_iota(jnp.int32, (8, 128), 0)
+    return jnp.where(row == 0, low, high)
+
+
+def entry_table(chosen, me, kv_count, own_blocks, per_dev):
+    slot_count = kv_count * CAP
+    spare = per_dev * NSEL
+    lane = lax.broadcasted_iota(jnp.int32, (NSEL, 128), 1)
+    entry = lax.broadcasted_iota(jnp.int32, (NSEL, 128), 0) + lane * NSEL
+    blocks = pltpu.roll(chosen, lax.rem(128 - me * per_dev + 128, 128), 1)
+    blocks = jnp.where(lane < per_dev, blocks, -1)
+    top = kv_count * own_blocks
+    lows = []
+    for o in range(kv_count):
+        inside = (blocks >= o * own_blocks) & (blocks < (o + 1) * own_blocks)
+        lows.append(jnp.min(jnp.where(inside, blocks, top), axis=0, keepdims=True))
+    low = jnp.min(jnp.concatenate(lows, axis=0), axis=1, keepdims=True)
+    slot = jnp.full((NSEL, 128), slot_count, jnp.int32)
+    for o in range(kv_count):
+        inside = (blocks >= o * own_blocks) & (blocks < (o + 1) * own_blocks)
+        at = o * CAP + jnp.where(blocks > low[o : o + 1], 1, 0)
+        slot = jnp.where(inside, at, slot)
+    mine = (blocks >= me * own_blocks) & (blocks < (me + 1) * own_blocks)
+    slot = jnp.where(mine, slot_count, slot)
+    places = []
+    for s in range(slot_count):
+        found = jnp.max(jnp.where(slot == s, entry, -1), axis=0, keepdims=True)
+        places.append(jnp.where(found < 0, spare, found))
+    return jnp.concatenate([jnp.minimum(slot, slot_count - 1), blocks] + places, axis=0)
+
+
+def finish_kernel(qg_ref, wg_ref, kvg_ref, qg_out, wg_out, kvg_out, sem):
+    pairs = ((qg_ref, qg_out), (wg_ref, wg_out), (kvg_ref, kvg_out))
+    copies = [pltpu.make_async_copy(src, dst, sem.at[i]) for i, (src, dst) in enumerate(pairs)]
+    for copy in copies:
+        copy.start()
+    for copy in copies:
+        copy.wait()
+
+
+def finish(*results):
+    hbm = pl.BlockSpec(memory_space=pl.ANY)
+    return pl.pallas_call(
+        finish_kernel,
+        out_shape=[jax.ShapeDtypeStruct(r.shape, r.dtype) for r in results],
+        in_specs=[hbm] * 3,
+        out_specs=[hbm] * 3,
+        scratch_shapes=[pltpu.SemaphoreType.DMA((3,))],
+        compiler_params=pltpu.CompilerParams(vmem_limit_bytes=1024 * 1024),
+        name="finish",
+    )(*results)
+
+
+def fused(kv_count, chosen, own_kv, log_sums, queries, out_grad, inputs):
+    operands = (chosen, own_kv, log_sums, queries, out_grad, inputs)
     tok_count, width = queries.shape
     per_dev = tok_count // QB
     rows = inputs.shape[1] // kv_count
@@ -443,24 +562,31 @@
         pltpu.VMEM((chunk_count, kv_count >> (k + 1), DH, rows), jnp.bfloat16) for k in range(bits)
     ]
     vmem = pl.BlockSpec(memory_space=pltpu.VMEM)
-    smem = pl.BlockSpec(memory_space=pltpu.SMEM)
     hbm = pl.BlockSpec(memory_space=pl.ANY)
     dma = pltpu.SemaphoreType.DMA
+    table_rows = 2 * NSEL + slot_count
     return pl.pallas_call(
         functools.partial(fused_kernel, kv_count, orders),
         out_shape=[
-            jax.ShapeDtypeStruct((tok_count, width), jnp.bfloat16),
-            jax.ShapeDtypeStruct((rows, width), jnp.float32),
-            jax.ShapeDtypeStruct((own_kv.shape[0], half, 2 * DH), jnp.float32),
-            jax.ShapeDtypeStruct((kv_count, CAP, half, 2 * DH), jnp.bfloat16),
+            pltpu.VMEM((tok_count, width), jnp.bfloat16),
+            pltpu.VMEM((rows, width), jnp.float32),
+            pltpu.VMEM((own_kv.shape[0], half, 2 * DH), jnp.float32),
         ],
-        in_specs=[smem] * 3 + [vmem] * 3 + [hbm] * 3,
-        out_specs=[vmem] * 4,
+        in_specs=[hbm] * 6,
+        out_specs=[vmem] * 3,
         scratch_shapes=[
+            pltpu.VMEM(chosen.shape, jnp.int32),
+            pltpu.VMEM((8, 128), jnp.int32),
+            pltpu.VMEM((table_rows, 128), jnp.int32),
+            pltpu.SMEM((8, 128), jnp.int32),
+            pltpu.SMEM((table_rows, 128), jnp.int32),
+            pltpu.VMEM((kv_count, CAP, KB, 2 * DH), jnp.bfloat16),
+            pltpu.VMEM(log_sums.shape, jnp.float32),
+            pltpu.VMEM(own_kv.shape, jnp.bfloat16),
             pltpu.VMEM((tok_count, width), jnp.bfloat16),
             pltpu.VMEM((tok_count, width), jnp.bfloat16),
             pltpu.VMEM(inputs.shape, jnp.bfloat16),
-            pltpu.VMEM((pool_count, KB, 2 * DH), jnp.bfloat16),
+            pltpu.VMEM((slot_count, KB, 2 * DH), jnp.bfloat16),
             pltpu.VMEM((per_dev, NSEL * KB, 2 * DH), jnp.bfloat16),
             pltpu.VMEM((per_dev, DH, NSEL * KB), jnp.bfloat16),
             pltpu.VMEM((per_dev * NSEL + 1, KB, 2 * DH), jnp.float32),
@@ -474,7 +600,7 @@
         + parts
         + parts
         + [
-            dma((3,)),
+            dma((8,)),
             dma((kv_count,)),
             dma((kv_count,)),
             dma,
@@ -485,83 +611,30 @@
             dma((chunk_count, bits)),
         ],
         compiler_params=pltpu.CompilerParams(
-            collective_id=0, has_side_effects=True, vmem_limit_bytes=60 * 1024 * 1024
+            collective_id=0, has_side_effects=True, vmem_limit_bytes=VMEM_LIMIT
         ),
         name="fused",
-    )(pool_index, block_list, place, outgoing, own_kv, log_sums, queries, out_grad, inputs)
+    )(*(pltpu.with_memory_space_constraint(x, pltpu.HBM) for x in operands))
 
 
 def fused_body(queries, keyvals, log_sums, out_grad, inputs, selection):
     kv_count = lax.axis_size("kv")
-    own_index = lax.axis_index("kv")
-    tok_count, width = queries.shape
-    per_dev = tok_count // QB
-    own_blocks = tok_count // KB
-    slot_count = kv_count * CAP
+    own_blocks = queries.shape[0] // KB
     own_kv = keyvals.reshape(own_blocks, KB, 2 * DH)
-    lists = selection.reshape(kv_count, per_dev * NSEL)
-    device_ids = jnp.arange(kv_count, dtype=jnp.int32)
-    mine = own_index * own_blocks + jnp.arange(own_blocks, dtype=jnp.int32)
-    wanted = jnp.any(lists[:, :, None] == mine[None, None, :], axis=1) & (
-        device_ids[:, None] != own_index
-    )
-    owner_slots = slot_table(wanted)
-    outgoing = jnp.einsum(
-        "rsb,bkc->rskc",
-        owner_slots.astype(jnp.bfloat16),
-        own_kv,
-        preferred_element_type=jnp.float32,
-    ).astype(jnp.bfloat16)
-    block_list = lax.dynamic_index_in_dim(lists, own_index, 0, keepdims=False)
-    every_block = jnp.arange(kv_count * own_blocks, dtype=jnp.int32)
-    hits = block_list[:, None] == every_block[None, :]
-    needed = jnp.any(hits, axis=0).reshape(kv_count, own_blocks) & (
-        device_ids[:, None] != own_index
-    )
-    slot_rank = jnp.cumsum(needed.astype(jnp.int32), axis=1) - 1
-    entry_rank = jnp.sum(jnp.where(hits, slot_rank.reshape(-1)[None, :], 0), axis=1)
-    safe_list = jnp.maximum(block_list, 0)
-    owner_index = safe_list // own_blocks
-    local_block = safe_list % own_blocks
-    pool_index = jnp.where(
-        owner_index == own_index, slot_count + local_block, owner_index * CAP + entry_rank
-    )
-    pool_index = jnp.where(block_list < 0, slot_count, pool_index)
-    entry_ids = jnp.arange(per_dev * NSEL, dtype=jnp.int32).reshape(1, per_dev, NSEL)
-    slot_ids = jnp.arange(slot_count, dtype=jnp.int32)[:, None, None]
-    spare = per_dev * NSEL
-    place = spare + jnp.sum(
-        jnp.where(pool_index.reshape(1, per_dev, NSEL) == slot_ids, entry_ids - spare, 0), axis=2
-    )
-    query_grad, weight_grad, own_grad, returned = fused(
-        kv_count,
-        pool_index,
-        block_list,
-        place.reshape(-1),
-        outgoing,
-        own_kv,
-        log_sums,
-        queries,
-        out_grad,
-        inputs,
-    )
-    keyval_grad = own_grad + jnp.einsum(
-        "rsb,rskc->bkc",
-        owner_slots.astype(jnp.bfloat16),
-        returned,
-        preferred_element_type=jnp.float32,
-    )
+    results = fused(kv_count, selection.T, own_kv, log_sums, queries, out_grad, inputs)
+    query_grad, weight_grad, keyval_grad = finish(*results)
     return (query_grad, keyval_grad, weight_grad)
 
 
-def fits(kv_count, tp_count, rows, width):
+def fits(kv_count, tp_count, tok_count, rows, width):
     power = kv_count & (kv_count - 1) == 0 and kv_count >= 8
-    return tp_count == 2 and power and rows % 128 == 0 and width % (2 * DH * GROUP) == 0
+    lanes = power and kv_count <= NSEL and kv_count * (tok_count // QB) <= 128
+    return tp_count == 2 and lanes and rows % 128 == 0 and width % (2 * DH * GROUP) == 0
 
 
 def step(queries, keyvals, log_sums, out_grad, inputs, selection):
     kv_count, tp_count = lax.axis_size("kv"), lax.axis_size("tp")
-    chosen = fits(kv_count, tp_count, inputs.shape[1] // kv_count, queries.shape[1])
+    chosen = fits(kv_count, tp_count, queries.shape[0], inputs.shape[1] // kv_count, queries.shape[1])
     return (fused_body if chosen else body)(
         queries, keyvals, log_sums, out_grad, inputs, selection
     )

time: 74.3 us -> 58.1 us (0.78)
  local copies, waits for them, and re-layouts: 6.91 us -> 0 us
  other arithmetic: 3.88 us -> 0 us
  Pallas kernels: 60.2 us -> 57.1 us
  matrix products: 2.29 us -> 0 us
    unnamed x5 -> x0, local copies, waits for them, and re-layouts: 4.63 us -> none
    pallas_call x1, Pallas kernels: 60.2 us -> 56 us  [fused(): pl.pallas_call(functools.partial(fused_kernel, kv_count, orders), out_sha...]
    dot_general x2 -> x0, matrix products: 2.29 us -> none  [the longest x1 1.16 us: fused_body(): jnp.einsum('rsb,bkc->rskc', owner_slots.astype(jnp.bfloat16), own_kv, pre...]
    add x3 -> x0, other arithmetic: 1.78 us -> none  [the longest x1 1.77 us: fused_body(): own_grad + jnp.einsum('rsb,rskc->bkc', owner_slots.astype(jnp.bfloat16),...]
    pallas_call x0 -> x1, Pallas kernels: none -> 1.1 us  [finish(): pl.pallas_call(finish_kernel, out_shape=[jax.ShapeDtypeStruct(r.shape, r....]
    dot_general x1 -> x0, local copies, waits for them, and re-layouts: 0.77 us -> none  [fused_body(): jnp.einsum('rsb,bkc->rskc', owner_slots.astype(jnp.bfloat16), own_kv, pre...]
    add x2 -> x0, local copies, waits for them, and re-layouts: 0.76 us -> none  [fused_body(): spare + jnp.sum(jnp.where(pool_index.reshape(1, per_dev, NSEL) == slot_id...]
where the time goes in v1:
time: 58.1 us; the launch traced here: 57.9 us
  Pallas kernels  57.1 us (98%)
  between operations  0.8 us (1%)
    pallas_call x1, Pallas kernels, fused(): pl.pallas_call(functools.partial(fused_kernel, kv_count, orders), out_sha...  56 us

profile of v1, /device:TPU:0, one launch (start us, length us, event | category | flops | bytes accessed | tf_op | source)
XLA Modules:
  0.0 57.9 jit_solution(7327115598489929494)
XLA Ops:
  0.6 56.0 %fused.1 = (bf16[896,512]{1,0:T(8,128)(2,1)S(1)}, f32[128,512]{1,0:T(8,128)S(1)}, f32[28,16,128]{2,1,0:T(8,128)S(1)}) custom-call(s32[16,112]{1,0:T(8,128)} %bitcast.3, bf16[28,32,128]{2,1,0:T(8,128)(2,1)} %bitcast.2, f32[8,896]{1,0:T(8,128)} %log_hbm.1, bf16[896,512]{1,0:T(8,128)(2,1)} %q_hbm.1, bf16[896,512]{1,0:T(8,128)(2,1)} %g_hbm.1, ...), custom_call_target="tpu_custom_call" | custom-call | tf_op jit(solution)/shard_map/fused/pallas_call | solution.py:568
  56.6 1.1 %finish.1 = (bf16[896,512]{1,0:T(8,128)(2,1)}, f32[128,512]{1,0:T(8,128)}, f32[28,16,128]{2,1,0:T(8,128)}) custom-call(bf16[896,512]{1,0:T(8,128)(2,1)S(1)} %get-tuple-element.9.qg_ref, f32[128,512]{1,0:T(8,128)S(1)} %get-tuple-element.10.wg_ref, f32[28,16,128]{2,1,0:T(8,128)S(1)} %get-tuple-element.11.kvg_ref), custom_call_target="tpu_custom_call" | custom-call | tf_op jit(solution)/shard_map/finish/pallas_call | solution.py:539

commit v2 on v1

--- a/solution.py
+++ b/solution.py
@@ -16,7 +16,9 @@
 DEAD = 1e30
 GROUP = 1
 UNROLL = True
-VMEM_LIMIT = 28 * 1024 * 1024
+PIECES = 8
+KEYS = 7
+VMEM_LIMIT = 48 * 1024 * 1024
 MESH = pl.DeviceIdType.MESH
 
 
@@ -181,8 +183,13 @@
     g_scr,
     in_scr,
     pool_scr,
-    kv_scr,
+    kk_scr,
+    vv_scr,
     kt_scr,
+    qm_scr,
+    gm_scr,
+    ds_scr,
+    pb_scr,
     dkv_scr,
     qgt_scr,
     total,
@@ -277,15 +284,33 @@
     later(lambda r: get_copy(r, me).start())
     for load in loads[2:5]:
         load.wait()
+    low_half = lax.broadcasted_iota(jnp.int32, (QB, 2 * DH), 1) < DH
+
+    def prepare(p, carry):
+        tok = pl.ds(pl.multiple_of(p * QB, QB), QB)
+        for pair in range(pair_count):
+            cols = slice(pair * 2 * DH, (pair + 1) * 2 * DH)
+            for src, dst, scale in ((q_scr, qm_scr, score_scale), (g_scr, gm_scr, 1.0)):
+                both = src[tok, cols] * jnp.asarray(scale, jnp.bfloat16)
+                zero = jnp.zeros_like(both)
+                at = pair * 2 * QB
+                dst[p, at : at + QB, :] = jnp.where(low_half, both, zero)
+                dst[p, at + QB : at + 2 * QB, :] = jnp.where(low_half, zero, both)
+        return carry
+
+    lax.fori_loop(0, per_dev, prepare, 0)
     loads[7].wait()
     earlier(lambda r: get_copy(me, r).wait_recv())
+    low_key = lax.broadcasted_iota(jnp.int32, (KB, 2 * DH), 1) < DH
 
     def gather(p, carry):
-        for e in range(diagonal):
-            kv_scr[p, e * KB : (e + 1) * KB, :] = own_scr[p * diagonal + e]
-        for e in range(diagonal, NSEL):
-            kv_scr[p, e * KB : (e + 1) * KB, :] = pool_scr[table_ref[e, p]]
-        kt_scr[p] = kv_scr[p][:, :DH].T
+        for e in range(NSEL):
+            rows = slice(e * KB, (e + 1) * KB)
+            both = own_scr[p * diagonal + e] if e < diagonal else pool_scr[table_ref[e, p]]
+            turned = jnp.concatenate([both[:, DH:], both[:, :DH]], axis=1)
+            kk_scr[p, rows, :] = jnp.where(low_key, both, turned)
+            vv_scr[p, rows, :] = jnp.where(low_key, turned, both)
+        kt_scr[p] = kk_scr[p][:, :DH].T * jnp.asarray(score_scale, jnp.bfloat16)
         return carry
 
     lax.fori_loop(0, per_dev, gather, 0)
@@ -295,54 +320,73 @@
     causal = key_row <= query_col
     nt = (((1,), (1,)), ((), ()))
 
-    def attend(group):
-        def block(p, carry):
-            tok = pl.ds(pl.multiple_of(p * QB, QB), QB)
-            keys = kv_scr[p, :, :DH]
-            values = kv_scr[p, :, DH:]
-            penalty = [
-                jnp.where(table_ref[NSEL + e, p] >= 0, jnp.float32(0.0), jnp.float32(DEAD))
-                for e in range(NSEL)
-            ]
-            dkv = None
-            for pair in range(group * GROUP, (group + 1) * GROUP):
-                at = pair * 2 * DH
-                q2 = jnp.concatenate([q_scr[tok, at : at + DH], q_scr[tok, at + DH : at + 2 * DH]], axis=0)
-                g2 = jnp.concatenate([g_scr[tok, at : at + DH], g_scr[tok, at + DH : at + 2 * DH]], axis=0)
-                log2 = jnp.concatenate(
-                    [log_ref[2 * pair : 2 * pair + 1, tok], log_ref[2 * pair + 1 : 2 * pair + 2, tok]], axis=1
-                )
-                log2 = log2 * LOG2E
-                scores = lax.dot_general(keys, q2, nt, preferred_element_type=jnp.float32)
-                dprob = lax.dot_general(values, g2, nt, preferred_element_type=jnp.float32)
-                shifted = jnp.concatenate(
-                    [
-                        scores[e * KB : (e + 1) * KB] * (score_scale * LOG2E) - (log2 + penalty[e])
-                        for e in range(NSEL)
-                    ],
-                    axis=0,
-                )
-                shifted = jnp.concatenate([jnp.where(causal, shifted[:QB], -DEAD), shifted[QB:]], axis=0)
-                prob = jnp.exp2(shifted)
-                prob_b = prob.astype(jnp.bfloat16)
-                delta = jnp.sum(prob_b.astype(jnp.float32) * dprob, axis=0, keepdims=True)
+    def attend(pair):
+        at = pair * 2 * DH
+        heads = slice(pair * 2 * QB, (pair + 1) * 2 * QB)
+        rows = NSEL * KB // 1
+
+        def multiply(p, h):
+            keys = slice(h * rows, (h + 1) * rows)
+            scores = lax.dot_general(
+                kk_scr[p, keys, :], qm_scr[p, heads, :], nt, preferred_element_type=jnp.float32
+            )
+            dprob = lax.dot_general(
+                vv_scr[p, keys, :], gm_scr[p, heads, :], nt, preferred_element_type=jnp.float32
+            )
+            return scores, dprob
+
+        def weigh(p, h, scores, dprob):
+            tok = slice(p * QB, (p + 1) * QB)
+            log2 = jnp.concatenate(
+                [log_ref[2 * pair : 2 * pair + 1, tok], log_ref[2 * pair + 1 : 2 * pair + 2, tok]], axis=1
+            )
+            log2 = log2 * LOG2E
+            parts = []
+            for i in range(rows // KB):
+                e = h * (rows // KB) + i
+                penalty = jnp.where(table_ref[NSEL + e, p] >= 0, jnp.float32(0.0), jnp.float32(DEAD))
+                part = scores[i * KB : (i + 1) * KB] * LOG2E - (log2 + penalty)
+                if e < diagonal:
+                    part = jnp.where(causal[e * KB : (e + 1) * KB], part, -DEAD)
+                parts.append(part)
+            prob = jnp.exp2(jnp.concatenate(parts, axis=0))
+            prob_b = prob.astype(jnp.bfloat16)
+            pb_scr[p, h * rows : (h + 1) * rows, heads] = prob_b
+            seen = prob_b.astype(jnp.float32)
+            delta = jnp.sum(seen * dprob, axis=0, keepdims=True)
+
+            return prob, delta
+
+        def finish_block(p, probs, dprobs, delta):
+            tok = slice(p * QB, (p + 1) * QB)
+            dq = None
+            for h in range(1):
+                keys = slice(h * rows, (h + 1) * rows)
+                prob, dprob = probs[h], dprobs[h]
                 dscore_b = (prob * (dprob - delta)).astype(jnp.bfloat16)
-                dq = jnp.dot(kt_scr[p], dscore_b, preferred_element_type=jnp.float32) * score_scale
-                dq = jnp.concatenate([dq[:, :QB], dq[:, QB:]], axis=0)
-                qgt_scr[at : at + 2 * DH, tok] = dq.astype(jnp.bfloat16)
-                qg_ref[tok, at : at + 2 * DH] = dq.T.astype(jnp.bfloat16)
-                dk = jnp.dot(dscore_b, q2, preferred_element_type=jnp.float32) * score_scale
-                dv = jnp.dot(prob_b, g2, preferred_element_type=jnp.float32)
-                part = jnp.concatenate([dk, dv], axis=1)
-                dkv = part if dkv is None else dkv + part
-            dkv = dkv.reshape(NSEL, KB, 2 * DH)
-            entries = pl.ds(p * NSEL, NSEL)
-            if group > 0:
-                dkv = dkv + dkv_scr[entries]
-            dkv_scr[entries] = dkv
-            return carry
-
-        lax.fori_loop(0, per_dev, block, 0, unroll=UNROLL)
+                ds_scr[p, keys, heads] = dscore_b
+            dq = jnp.dot(kt_scr[p], ds_scr[p, :, heads], preferred_element_type=jnp.float32)
+            dq = jnp.concatenate([dq[:, :QB], dq[:, QB:]], axis=0)
+            qgt_scr[at : at + 2 * DH, tok] = dq.astype(jnp.bfloat16)
+            qg_ref[tok, at : at + 2 * DH] = dq.T.astype(jnp.bfloat16)
+
+        ready = multiply(0, 0)
+        for p in range(per_dev):
+            now = ready
+            ready = multiply(p + 1, 0) if p + 1 < per_dev else None
+            prob, delta = weigh(p, 0, *now)
+            finish_block(p, [prob], [now[1]], delta)
+
+    low_row = lax.broadcasted_iota(jnp.int32, (NSEL * KB, 2 * DH), 1) < DH
+
+    def key_value(p, carry):
+        dk = jnp.dot(ds_scr[p], qm_scr[p], preferred_element_type=jnp.float32)
+        dv = jnp.dot(pb_scr[p], gm_scr[p], preferred_element_type=jnp.float32)
+        near = jnp.where(low_row, dk, dv)
+        far = jnp.where(low_row, dv, dk)
+        dkv = near + pltpu.roll(far, DH, 1)
+        dkv_scr[pl.ds(p * NSEL, NSEL)] = dkv.reshape(NSEL, KB, 2 * DH)
+        return carry
 
     def product(pair):
         cols = slice(pair * GROUP * 2 * DH, (pair + 1) * GROUP * 2 * DH)
@@ -356,7 +400,7 @@
             total[2 * j + 1, cols, :] = part[:, rows:]
             return carry
 
-        lax.fori_loop(0, kv_count // 2, piece, 0)
+        lax.fori_loop(0, kv_count // 2, piece, 0, unroll=PIECES)
 
     def owner_of(c, slot):
         owner = me
@@ -435,15 +479,16 @@
         attend(pair)
         if pair == 0:
             loads[5].wait()
-        if pair == pair_count - 1:
-            lax.fori_loop(0, slot_count, collect, 0)
-            for p in range(per_dev):
-                at = slot_count + p * diagonal
-                half_scr[0, at : at + diagonal] = dkv_scr[p * NSEL : p * NSEL + diagonal, :half, :]
-                half_scr[1, at : at + diagonal] = dkv_scr[p * NSEL : p * NSEL + diagonal, half:, :]
-            tp_copy.start()
         product(pair)
         advance(pair)
+    lax.fori_loop(0, per_dev, key_value, 0, unroll=KEYS)
+    lax.fori_loop(0, slot_count, collect, 0)
+    for p in range(per_dev):
+        at = slot_count + p * diagonal
+        half_scr[0, at : at + diagonal] = dkv_scr[p * NSEL : p * NSEL + diagonal, :half, :]
+        half_scr[1, at : at + diagonal] = dkv_scr[p * NSEL : p * NSEL + diagonal, half:, :]
+    tp_copy.start()
+    advance(pair_count)
 
     tp_copy.wait_recv()
     mine = half_scr.at[core]
@@ -455,7 +500,7 @@
     earlier(lambda r: ret_copy(r, me).start())
     own_sum = (mine[slot_count:] + tp_scr[slot_count:]).reshape(own_blocks * half, 2 * DH)
 
-    for turn in range(pair_count, pair_count + bits):
+    for turn in range(pair_count + 1, pair_count + bits):
         advance(turn)
     later(lambda r: ret_copy(me, r).wait_recv())
     column = lax.broadcasted_iota(jnp.int32, (1, slot_count * half), 1)
@@ -588,7 +633,12 @@
             pltpu.VMEM(inputs.shape, jnp.bfloat16),
             pltpu.VMEM((slot_count, KB, 2 * DH), jnp.bfloat16),
             pltpu.VMEM((per_dev, NSEL * KB, 2 * DH), jnp.bfloat16),
+            pltpu.VMEM((per_dev, NSEL * KB, 2 * DH), jnp.bfloat16),
             pltpu.VMEM((per_dev, DH, NSEL * KB), jnp.bfloat16),
+            pltpu.VMEM((per_dev, QB * width // DH, 2 * DH), jnp.bfloat16),
+            pltpu.VMEM((per_dev, QB * width // DH, 2 * DH), jnp.bfloat16),
+            pltpu.VMEM((per_dev, NSEL * KB, QB * width // DH), jnp.bfloat16),
+            pltpu.VMEM((per_dev, NSEL * KB, QB * width // DH), jnp.bfloat16),
             pltpu.VMEM((per_dev * NSEL + 1, KB, 2 * DH), jnp.float32),
             pltpu.VMEM((width, tok_count), jnp.bfloat16),
             pltpu.VMEM((kv_count, width, rows), jnp.float32),

time: 58.1 us -> 49.7 us (0.86)
  Pallas kernels: 57.1 us -> 48.8 us
    pallas_call x1, Pallas kernels: 56 us -> 47.7 us  [fused(): pl.pallas_call(functools.partial(fused_kernel, kv_count, orders), out_sha...]
where the time goes in v2:
time: 49.7 us; the launch traced here: 49.5 us
  Pallas kernels  48.8 us (98%)
  between operations  0.64 us (1%)
    pallas_call x1, Pallas kernels, fused(): pl.pallas_call(functools.partial(fused_kernel, kv_count, orders), out_sha...  47.7 us
    pallas_call x1, Pallas kernels, finish(): pl.pallas_call(finish_kernel, out_shape=[jax.ShapeDtypeStruct(r.shape, r....  1.1 us

profile of v2, /device:TPU:0, one launch (start us, length us, event | category | flops | bytes accessed | tf_op | source)
XLA Modules:
  0.0 49.5 jit_solution(7727382616968461989)
XLA Ops:
  0.6 47.7 %fused.1 = (bf16[896,512]{1,0:T(8,128)(2,1)S(1)}, f32[128,512]{1,0:T(8,128)S(1)}, f32[28,16,128]{2,1,0:T(8,128)S(1)}) custom-call(s32[16,112]{1,0:T(8,128)} %bitcast.3, bf16[28,32,128]{2,1,0:T(8,128)(2,1)} %bitcast.2, f32[8,896]{1,0:T(8,128)} %log_hbm.1, bf16[896,512]{1,0:T(8,128)(2,1)} %q_hbm.1, bf16[896,512]{1,0:T(8,128)(2,1)} %g_hbm.1, ...), custom_call_target="tpu_custom_call" | custom-call | tf_op jit(solution)/shard_map/fused/pallas_call | solution.py:613
  48.4 1.1 %finish.1 = (bf16[896,512]{1,0:T(8,128)(2,1)}, f32[128,512]{1,0:T(8,128)}, f32[28,16,128]{2,1,0:T(8,128)}) custom-call(bf16[896,512]{1,0:T(8,128)(2,1)S(1)} %get-tuple-element.9.qg_ref, f32[128,512]{1,0:T(8,128)S(1)} %get-tuple-element.10.wg_ref, f32[28,16,128]{2,1,0:T(8,128)S(1)} %get-tuple-element.11.kvg_ref), custom_call_target="tpu_custom_call" | custom-call | tf_op jit(solution)/shard_map/finish/pallas_call | solution.py:584

commit v3 on v2

--- a/solution.py
+++ b/solution.py
@@ -17,6 +17,11 @@
 GROUP = 1
 UNROLL = True
 PIECES = 8
+HOP_US = (5.5, 4.0, 3.5, 4.0)
+LAST_US = (5.5, 4.0, 3.5, 4.0)
+PAIR_US = 2.95
+KEY_US = 0.78
+TP_US = 7.4
 KEYS = 7
 VMEM_LIMIT = 48 * 1024 * 1024
 MESH = pl.DeviceIdType.MESH
@@ -152,6 +157,31 @@
         first = [0, 1, 2]
         orders.append(first[turn:] + first[:turn] + list(range(3, bits)))
     return orders
+
+
+def plan(pair_count, per_dev, bits):
+    points = []
+    for pair in range(pair_count):
+        points += [("mid", pair, PAIR_US * (pair + 0.5)), ("end", pair, PAIR_US * (pair + 1))]
+    last = PAIR_US * pair_count
+    points += [("key", p, last + KEY_US * (p + 1)) for p in range(per_dev)]
+    chosen, sends, finals = {}, [], []
+    for pair in range(pair_count):
+        hops = LAST_US if pair == pair_count - 1 else HOP_US
+        lags = hops[: bits - 1] + hops[-1:]
+        chosen.setdefault(("end", pair), []).append((pair, 0))
+        ready = PAIR_US * (pair + 1)
+        for k, lag in enumerate(lags):
+            ready += lag
+            fitting = [point for point in points if point[2] >= ready]
+            if fitting and k + 1 < len(lags):
+                chosen.setdefault(fitting[0][:2], []).append((pair, k + 1))
+                ready = fitting[0][2]
+            elif k + 1 < len(lags):
+                sends.append((ready - last, pair, k + 1))
+            else:
+                finals.append((ready - last, pair, k + 1))
+    return chosen, sorted(sends), finals
 
 
 def flip(index, place):
@@ -237,8 +267,8 @@
     ]
     for load in loads[:6]:
         load.start()
-    pool_scr[...] = jnp.zeros(pool_scr.shape, jnp.bfloat16)
-    ret_scr[...] = jnp.zeros(ret_scr.shape, jnp.bfloat16)
+    pool_scr[me] = jnp.zeros(pool_scr.shape[1:], jnp.bfloat16)
+    ret_scr[me] = jnp.zeros(ret_scr.shape[1:], jnp.bfloat16)
 
     barrier = pltpu.get_barrier_semaphore()
     for step in range(1, kv_count):
@@ -259,29 +289,26 @@
             out_scr[r, s] = own_scr[first_ref[s, r * per_dev]]
     pl.semaphore_wait(barrier, kv_count)
 
-    def get_copy(target, source):
-        return pltpu.make_async_remote_copy(
-            src_ref=out_scr.at[target],
-            dst_ref=pool_scr.at[pl.ds(source * CAP, CAP)],
-            send_sem=get_send.at[target],
-            recv_sem=get_recv.at[source],
-            device_id=(target, core),
-            device_id_type=MESH,
-        )
-
-    def later(do):
-        for step in range(kv_count - 1, 0, -1):
-            @pl.when(me + step < kv_count)
-            def _():
-                do(me + step)
-
-    def earlier(do):
-        for step in range(1, kv_count):
-            @pl.when(me >= step)
-            def _():
-                do(me - step)
-
-    later(lambda r: get_copy(r, me).start())
+    def exchange(send, receive, sems):
+        def copy(src_ref, dst_ref, target):
+            return pltpu.make_async_remote_copy(
+                src_ref=src_ref,
+                dst_ref=dst_ref,
+                send_sem=sems[0],
+                recv_sem=sems[1],
+                device_id=(target, core),
+                device_id_type=MESH,
+            )
+
+        def start():
+            for step in range(kv_count - 1, 0, -1):
+                copy(send.at[peer(step)], receive.at[me], peer(step)).start()
+
+        every = copy(send.at[: kv_count - 1], receive.at[: kv_count - 1], peer(1))
+        return start, every
+
+    get_start, get_every = exchange(out_scr, pool_scr, (get_send, get_recv))
+    get_start()
     for load in loads[2:5]:
         load.wait()
     low_half = lax.broadcasted_iota(jnp.int32, (QB, 2 * DH), 1) < DH
@@ -299,21 +326,25 @@
         return carry
 
     lax.fori_loop(0, per_dev, prepare, 0)
+    low_key = lax.broadcasted_iota(jnp.int32, (KB, 2 * DH), 1) < DH
+    key_scale = jnp.asarray(score_scale, jnp.bfloat16)
+
+    def spread_block(p, e, both):
+        rows = slice(e * KB, (e + 1) * KB)
+        turned = jnp.concatenate([both[:, DH:], both[:, :DH]], axis=1)
+        kk_scr[p, rows, :] = jnp.where(low_key, both, turned)
+        vv_scr[p, rows, :] = jnp.where(low_key, turned, both)
+
+    for p in range(per_dev):
+        for e in range(diagonal):
+            spread_block(p, e, own_scr[p * diagonal + e])
+        kt_scr[p, :, :QB] = kk_scr[p, :QB, :DH].T * key_scale
     loads[7].wait()
-    earlier(lambda r: get_copy(me, r).wait_recv())
-    low_key = lax.broadcasted_iota(jnp.int32, (KB, 2 * DH), 1) < DH
-
-    def gather(p, carry):
-        for e in range(NSEL):
-            rows = slice(e * KB, (e + 1) * KB)
-            both = own_scr[p * diagonal + e] if e < diagonal else pool_scr[table_ref[e, p]]
-            turned = jnp.concatenate([both[:, DH:], both[:, :DH]], axis=1)
-            kk_scr[p, rows, :] = jnp.where(low_key, both, turned)
-            vv_scr[p, rows, :] = jnp.where(low_key, turned, both)
-        kt_scr[p] = kk_scr[p][:, :DH].T * jnp.asarray(score_scale, jnp.bfloat16)
-        return carry
-
-    lax.fori_loop(0, per_dev, gather, 0)
+    get_every.wait_recv()
+    for p in range(per_dev):
+        for e in range(diagonal, NSEL):
+            spread_block(p, e, pool_scr[table_ref[e, p], table_ref[2 * NSEL + slot_count + e, p]])
+        kt_scr[p, :, QB:] = kk_scr[p, QB:, :DH].T * key_scale
 
     key_row = lax.broadcasted_iota(jnp.int32, (QB, 2 * QB), 0)
     query_col = lax.broadcasted_iota(jnp.int32, (QB, 2 * QB), 1) % QB
@@ -376,17 +407,18 @@
             ready = multiply(p + 1, 0) if p + 1 < per_dev else None
             prob, delta = weigh(p, 0, *now)
             finish_block(p, [prob], [now[1]], delta)
+            if p == per_dev // 2:
+                advance("mid", pair)
 
     low_row = lax.broadcasted_iota(jnp.int32, (NSEL * KB, 2 * DH), 1) < DH
 
-    def key_value(p, carry):
+    def key_value(p):
         dk = jnp.dot(ds_scr[p], qm_scr[p], preferred_element_type=jnp.float32)
         dv = jnp.dot(pb_scr[p], gm_scr[p], preferred_element_type=jnp.float32)
         near = jnp.where(low_row, dk, dv)
         far = jnp.where(low_row, dv, dk)
         dkv = near + pltpu.roll(far, DH, 1)
-        dkv_scr[pl.ds(p * NSEL, NSEL)] = dkv.reshape(NSEL, KB, 2 * DH)
-        return carry
+        dkv_scr[p * NSEL : (p + 1) * NSEL] = dkv.reshape(NSEL, KB, 2 * DH)
 
     def product(pair):
         cols = slice(pair * GROUP * 2 * DH, (pair + 1) * GROUP * 2 * DH)
@@ -421,20 +453,24 @@
         return pltpu.make_async_remote_copy(
             src_ref=send_scr[k].at[c],
             dst_ref=recv_scr[k].at[c],
-            send_sem=w_send.at[c, k],
+            send_sem=w_send.at[c],
             recv_sem=w_recv.at[c, k],
             device_id=(flip(me, orders[c][k]), core),
             device_id_type=MESH,
         )
+
+    def place(c, value):
+        wg_ref[:, c * DH : (c + 1) * DH] = value.T
 
     def weight_stage(pair, k):
         left = kv_count >> (k + 1)
         for c in range(2 * GROUP * pair, 2 * GROUP * (pair + 1)):
             if k > 0:
                 weight_copy(c, k - 1).wait_recv()
+                weight_copy(c, k - 1).wait_send()
             if k == bits:
                 value = total[me, c * DH : (c + 1) * DH, :] + recv_scr[k - 1][c, 0].astype(jnp.float32)
-                wg_ref[:, c * DH : (c + 1) * DH] = value.T
+                place(c, value)
                 continue
             for slot in range(left, 2 * left):
                 send_scr[k][c, slot - left] = current(c, slot, k).astype(jnp.bfloat16)
@@ -443,10 +479,9 @@
                 for slot in range(left):
                     current(c, slot, k)
 
-    def advance(turn):
-        for k in range(bits + 1):
-            if 0 <= turn - k < pair_count:
-                weight_stage(turn - k, k)
+    def advance(*point):
+        for pair, k in chosen.get(point, ()):
+            weight_stage(pair, k)
 
     tp_copy = pltpu.make_async_remote_copy(
         src_ref=half_scr.at[other],
@@ -457,15 +492,7 @@
         device_id_type=MESH,
     )
 
-    def ret_copy(target, source):
-        return pltpu.make_async_remote_copy(
-            src_ref=slot_scr.at[target],
-            dst_ref=ret_scr.at[source],
-            send_sem=ret_send.at[target],
-            recv_sem=ret_recv.at[source],
-            device_id=(target, core),
-            device_id_type=MESH,
-        )
+    ret_start, ret_every = exchange(slot_scr, ret_scr, (ret_send, ret_recv))
 
     def collect(s, carry):
         value = dkv_scr[table_ref[2 * NSEL + s, 0]]
@@ -475,20 +502,25 @@
         half_scr[1, s] = value[half:]
         return carry
 
+    chosen, sends, finals = plan(pair_count, per_dev, bits)
     for pair in range(pair_count):
         attend(pair)
         if pair == 0:
             loads[5].wait()
         product(pair)
-        advance(pair)
-    lax.fori_loop(0, per_dev, key_value, 0, unroll=KEYS)
+        advance("end", pair)
+    for p in range(per_dev):
+        key_value(p)
+        advance("key", p)
     lax.fori_loop(0, slot_count, collect, 0)
     for p in range(per_dev):
         at = slot_count + p * diagonal
         half_scr[0, at : at + diagonal] = dkv_scr[p * NSEL : p * NSEL + diagonal, :half, :]
         half_scr[1, at : at + diagonal] = dkv_scr[p * NSEL : p * NSEL + diagonal, half:, :]
     tp_copy.start()
-    advance(pair_count)
+    for ready, pair, k in sends:
+        if ready < TP_US:
+            weight_stage(pair, k)
 
     tp_copy.wait_recv()
     mine = half_scr.at[core]
@@ -497,12 +529,15 @@
         .astype(jnp.bfloat16)
         .reshape(kv_count, CAP, half, 2 * DH)
     )
-    earlier(lambda r: ret_copy(r, me).start())
+    ret_start()
     own_sum = (mine[slot_count:] + tp_scr[slot_count:]).reshape(own_blocks * half, 2 * DH)
 
-    for turn in range(pair_count + 1, pair_count + bits):
-        advance(turn)
-    later(lambda r: ret_copy(me, r).wait_recv())
+    for ready, pair, k in sends:
+        if ready >= TP_US:
+            weight_stage(pair, k)
+    for ready, pair, k in finals[:-1]:
+        weight_stage(pair, k)
+    ret_every.wait_recv()
     column = lax.broadcasted_iota(jnp.int32, (1, slot_count * half), 1)
     block = jnp.zeros(column.shape, jnp.int32)
     for r in range(kv_count):
@@ -514,12 +549,11 @@
     back = ret_scr[...].reshape(slot_count * half, 2 * DH)
     kvg = own_sum + jnp.dot(spread, back, preferred_element_type=jnp.float32)
     kvg_ref[...] = kvg.reshape(own_blocks, half, 2 * DH)
-    later(lambda r: get_copy(r, me).wait_send())
-    earlier(lambda r: ret_copy(r, me).wait_send())
+    get_every.wait_send()
+    ret_every.wait_send()
     tp_copy.wait_send()
-    for c in range(chunk_count):
-        for k in range(bits):
-            weight_copy(c, k).wait_send()
+    for ready, pair, k in finals[-1:]:
+        weight_stage(pair, k)
 
 
 def padded(chosen):
@@ -567,7 +601,8 @@
     for s in range(slot_count):
         found = jnp.max(jnp.where(slot == s, entry, -1), axis=0, keepdims=True)
         places.append(jnp.where(found < 0, spare, found))
-    return jnp.concatenate([jnp.minimum(slot, slot_count - 1), blocks] + places, axis=0)
+    used = jnp.minimum(slot, slot_count - 1)
+    return jnp.concatenate([used // CAP, blocks] + places + [used % CAP], axis=0)
 
 
 def finish_kernel(qg_ref, wg_ref, kvg_ref, qg_out, wg_out, kvg_out, sem):
@@ -609,7 +644,7 @@
     vmem = pl.BlockSpec(memory_space=pltpu.VMEM)
     hbm = pl.BlockSpec(memory_space=pl.ANY)
     dma = pltpu.SemaphoreType.DMA
-    table_rows = 2 * NSEL + slot_count
+    table_rows = 3 * NSEL + slot_count
     return pl.pallas_call(
         functools.partial(fused_kernel, kv_count, orders),
         out_shape=[
@@ -631,7 +666,7 @@
             pltpu.VMEM((tok_count, width), jnp.bfloat16),
             pltpu.VMEM((tok_count, width), jnp.bfloat16),
             pltpu.VMEM(inputs.shape, jnp.bfloat16),
-            pltpu.VMEM((slot_count, KB, 2 * DH), jnp.bfloat16),
+            pltpu.VMEM((kv_count, CAP, KB, 2 * DH), jnp.bfloat16),
             pltpu.VMEM((per_dev, NSEL * KB, 2 * DH), jnp.bfloat16),
             pltpu.VMEM((per_dev, NSEL * KB, 2 * DH), jnp.bfloat16),
             pltpu.VMEM((per_dev, DH, NSEL * KB), jnp.bfloat16),
@@ -651,13 +686,13 @@
         + parts
         + [
             dma((8,)),
-            dma((kv_count,)),
-            dma((kv_count,)),
             dma,
             dma,
-            dma((kv_count,)),
-            dma((kv_count,)),
-            dma((chunk_count, bits)),
+            dma,
+            dma,
+            dma,
+            dma,
+            dma((chunk_count,)),
             dma((chunk_count, bits)),
         ],
         compiler_params=pltpu.CompilerParams(

time: 49.7 us -> 44.8 us (0.901)
  Pallas kernels: 48.8 us -> 43.8 us
    pallas_call x1, Pallas kernels: 47.7 us -> 42.7 us  [fused(): pl.pallas_call(functools.partial(fused_kernel, kv_count, orders), out_sha...]
where the time goes in v3:
time: 44.8 us; the launch traced here: 44.6 us
  Pallas kernels  43.8 us (98%)
  between operations  0.8 us (2%)
    pallas_call x1, Pallas kernels, fused(): pl.pallas_call(functools.partial(fused_kernel, kv_count, orders), out_sha...  42.7 us
    pallas_call x1, Pallas kernels, finish(): pl.pallas_call(finish_kernel, out_shape=[jax.ShapeDtypeStruct(r.shape, r....  1.1 us

profile of v3, /device:TPU:0, one launch (start us, length us, event | category | flops | bytes accessed | tf_op | source)
XLA Modules:
  0.0 44.6 jit_solution(1523342419312609927)
XLA Ops:
  0.6 42.7 %fused.1 = (bf16[896,512]{1,0:T(8,128)(2,1)S(1)}, f32[128,512]{1,0:T(8,128)S(1)}, f32[28,16,128]{2,1,0:T(8,128)S(1)}) custom-call(s32[16,112]{1,0:T(8,128)} %bitcast.3, bf16[28,32,128]{2,1,0:T(8,128)(2,1)} %bitcast.2, f32[8,896]{1,0:T(8,128)} %log_hbm.1, bf16[896,512]{1,0:T(8,128)(2,1)} %q_hbm.1, bf16[896,512]{1,0:T(8,128)(2,1)} %g_hbm.1, ...), custom_call_target="tpu_custom_call" | custom-call | tf_op jit(solution)/shard_map/fused/pallas_call | solution.py:648
  43.3 1.1 %finish.1 = (bf16[896,512]{1,0:T(8,128)(2,1)}, f32[128,512]{1,0:T(8,128)}, f32[28,16,128]{2,1,0:T(8,128)}) custom-call(bf16[896,512]{1,0:T(8,128)(2,1)S(1)} %get-tuple-element.9.qg_ref, f32[128,512]{1,0:T(8,128)S(1)} %get-tuple-element.10.wg_ref, f32[28,16,128]{2,1,0:T(8,128)S(1)} %get-tuple-element.11.kvg_ref), custom_call_target="tpu_custom_call" | custom-call | tf_op jit(solution)/shard_map/finish/pallas_call | solution.py:619

commit v4 on v3

--- a/solution.py
+++ b/solution.py
@@ -19,11 +19,11 @@
 PIECES = 8
 HOP_US = (5.5, 4.0, 3.5, 4.0)
 LAST_US = (5.5, 4.0, 3.5, 4.0)
-PAIR_US = 2.95
+PAIR_US = 2.6
 KEY_US = 0.78
 TP_US = 7.4
 KEYS = 7
-VMEM_LIMIT = 48 * 1024 * 1024
+VMEM_LIMIT = 56 * 1024 * 1024
 MESH = pl.DeviceIdType.MESH
 
 
@@ -220,6 +220,9 @@
     gm_scr,
     ds_scr,
     pb_scr,
+    near_prob,
+    near_dprob,
+    near_delta,
     dkv_scr,
     qgt_scr,
     total,
@@ -339,6 +342,52 @@
         for e in range(diagonal):
             spread_block(p, e, own_scr[p * diagonal + e])
         kt_scr[p, :, :QB] = kk_scr[p, :QB, :DH].T * key_scale
+    key_row = lax.broadcasted_iota(jnp.int32, (QB, 2 * QB), 0)
+    query_col = lax.broadcasted_iota(jnp.int32, (QB, 2 * QB), 1) % QB
+    causal = key_row <= query_col
+    nt = (((1,), (1,)), ((), ()))
+
+    def multiply(p, pair, first, last):
+        heads = slice(pair * 2 * QB, (pair + 1) * 2 * QB)
+        scores = lax.dot_general(
+            kk_scr[p, first:last, :], qm_scr[p, heads, :], nt, preferred_element_type=jnp.float32
+        )
+        dprob = lax.dot_general(
+            vv_scr[p, first:last, :], gm_scr[p, heads, :], nt, preferred_element_type=jnp.float32
+        )
+        return scores, dprob
+
+    def weigh(p, pair, first, last, scores, dprob):
+        tok = slice(p * QB, (p + 1) * QB)
+        heads = slice(pair * 2 * QB, (pair + 1) * 2 * QB)
+        log2 = jnp.concatenate(
+            [log_ref[2 * pair : 2 * pair + 1, tok], log_ref[2 * pair + 1 : 2 * pair + 2, tok]], axis=1
+        )
+        log2 = log2 * LOG2E
+        parts = []
+        for e in range(first, last):
+            part = scores[(e - first) * KB : (e - first + 1) * KB] * LOG2E
+            if e < diagonal:
+                part = jnp.where(causal[e * KB : (e + 1) * KB], part - log2, -DEAD)
+            else:
+                penalty = jnp.where(table_ref[NSEL + e, p] >= 0, jnp.float32(0.0), jnp.float32(DEAD))
+                part = part - (log2 + penalty)
+            parts.append(part)
+        prob = jnp.exp2(jnp.concatenate(parts, axis=0))
+        prob_b = prob.astype(jnp.bfloat16)
+        pb_scr[p, first * KB : last * KB, heads] = prob_b
+        delta = jnp.sum(prob_b.astype(jnp.float32) * dprob, axis=0, keepdims=True)
+        return prob, delta
+
+    steps = [(p, pair) for p in range(per_dev) for pair in range(pair_count)]
+    ready = multiply(*steps[0], 0, QB)
+    for i, (p, pair) in enumerate(steps):
+        now = ready
+        ready = multiply(*steps[i + 1], 0, QB) if i + 1 < len(steps) else None
+        prob, delta = weigh(p, pair, 0, diagonal, *now)
+        near_prob[i] = prob
+        near_dprob[i] = now[1]
+        near_delta[i] = jnp.broadcast_to(delta, near_delta.shape[1:])
     loads[7].wait()
     get_every.wait_recv()
     for p in range(per_dev):
@@ -346,67 +395,29 @@
             spread_block(p, e, pool_scr[table_ref[e, p], table_ref[2 * NSEL + slot_count + e, p]])
         kt_scr[p, :, QB:] = kk_scr[p, QB:, :DH].T * key_scale
 
-    key_row = lax.broadcasted_iota(jnp.int32, (QB, 2 * QB), 0)
-    query_col = lax.broadcasted_iota(jnp.int32, (QB, 2 * QB), 1) % QB
-    causal = key_row <= query_col
-    nt = (((1,), (1,)), ((), ()))
-
     def attend(pair):
         at = pair * 2 * DH
         heads = slice(pair * 2 * QB, (pair + 1) * 2 * QB)
-        rows = NSEL * KB // 1
-
-        def multiply(p, h):
-            keys = slice(h * rows, (h + 1) * rows)
-            scores = lax.dot_general(
-                kk_scr[p, keys, :], qm_scr[p, heads, :], nt, preferred_element_type=jnp.float32
-            )
-            dprob = lax.dot_general(
-                vv_scr[p, keys, :], gm_scr[p, heads, :], nt, preferred_element_type=jnp.float32
-            )
-            return scores, dprob
-
-        def weigh(p, h, scores, dprob):
+
+        def finish_block(p, prob, dprob, delta):
             tok = slice(p * QB, (p + 1) * QB)
-            log2 = jnp.concatenate(
-                [log_ref[2 * pair : 2 * pair + 1, tok], log_ref[2 * pair + 1 : 2 * pair + 2, tok]], axis=1
-            )
-            log2 = log2 * LOG2E
-            parts = []
-            for i in range(rows // KB):
-                e = h * (rows // KB) + i
-                penalty = jnp.where(table_ref[NSEL + e, p] >= 0, jnp.float32(0.0), jnp.float32(DEAD))
-                part = scores[i * KB : (i + 1) * KB] * LOG2E - (log2 + penalty)
-                if e < diagonal:
-                    part = jnp.where(causal[e * KB : (e + 1) * KB], part, -DEAD)
-                parts.append(part)
-            prob = jnp.exp2(jnp.concatenate(parts, axis=0))
-            prob_b = prob.astype(jnp.bfloat16)
-            pb_scr[p, h * rows : (h + 1) * rows, heads] = prob_b
-            seen = prob_b.astype(jnp.float32)
-            delta = jnp.sum(seen * dprob, axis=0, keepdims=True)
-
-            return prob, delta
-
-        def finish_block(p, probs, dprobs, delta):
-            tok = slice(p * QB, (p + 1) * QB)
-            dq = None
-            for h in range(1):
-                keys = slice(h * rows, (h + 1) * rows)
-                prob, dprob = probs[h], dprobs[h]
-                dscore_b = (prob * (dprob - delta)).astype(jnp.bfloat16)
-                ds_scr[p, keys, heads] = dscore_b
-            dq = jnp.dot(kt_scr[p], ds_scr[p, :, heads], preferred_element_type=jnp.float32)
+            slot = p * pair_count + pair
+            delta = delta + near_delta[slot][:1]
+            near = near_prob[slot] * (near_dprob[slot] - delta)
+            far = prob * (dprob - delta)
+            dscore_b = jnp.concatenate([near, far], axis=0).astype(jnp.bfloat16)
+            ds_scr[p, :, heads] = dscore_b
+            dq = jnp.dot(kt_scr[p], dscore_b, preferred_element_type=jnp.float32)
             dq = jnp.concatenate([dq[:, :QB], dq[:, QB:]], axis=0)
             qgt_scr[at : at + 2 * DH, tok] = dq.astype(jnp.bfloat16)
             qg_ref[tok, at : at + 2 * DH] = dq.T.astype(jnp.bfloat16)
 
-        ready = multiply(0, 0)
+        ready = multiply(0, pair, QB, NSEL * KB)
         for p in range(per_dev):
             now = ready
-            ready = multiply(p + 1, 0) if p + 1 < per_dev else None
-            prob, delta = weigh(p, 0, *now)
-            finish_block(p, [prob], [now[1]], delta)
+            ready = multiply(p + 1, pair, QB, NSEL * KB) if p + 1 < per_dev else None
+            prob, delta = weigh(p, pair, diagonal, NSEL, *now)
+            finish_block(p, prob, now[1], delta)
             if p == per_dev // 2:
                 advance("mid", pair)
 
@@ -674,6 +685,9 @@
             pltpu.VMEM((per_dev, QB * width // DH, 2 * DH), jnp.bfloat16),
             pltpu.VMEM((per_dev, NSEL * KB, QB * width // DH), jnp.bfloat16),
             pltpu.VMEM((per_dev, NSEL * KB, QB * width // DH), jnp.bfloat16),
+            pltpu.VMEM((per_dev * chunk_count // 2, QB, 2 * QB), jnp.float32),
+            pltpu.VMEM((per_dev * chunk_count // 2, QB, 2 * QB), jnp.float32),
+            pltpu.VMEM((per_dev * chunk_count // 2, 8, 2 * QB), jnp.float32),
             pltpu.VMEM((per_dev * NSEL + 1, KB, 2 * DH), jnp.float32),
             pltpu.VMEM((width, tok_count), jnp.bfloat16),
             pltpu.VMEM((kv_count, width, rows), jnp.float32),

time: 44.8 us -> 44.4 us (level)
  Pallas kernels: 43.8 us -> 43.3 us
    pallas_call x1, Pallas kernels: 42.7 us -> 42.2 us  [fused(): pl.pallas_call(functools.partial(fused_kernel, kv_count, orders), out_sha...]
where the time goes in v4:
time: 44.4 us; the launch traced here: 44.1 us
  Pallas kernels  43.3 us (98%)
  between operations  0.8 us (2%)
    pallas_call x1, Pallas kernels, fused(): pl.pallas_call(functools.partial(fused_kernel, kv_count, orders), out_sha...  42.2 us
    pallas_call x1, Pallas kernels, finish(): pl.pallas_call(finish_kernel, out_shape=[jax.ShapeDtypeStruct(r.shape, r....  1.1 us

profile of v4, /device:TPU:0, one launch (start us, length us, event | category | flops | bytes accessed | tf_op | source)
XLA Modules:
  0.0 44.1 jit_solution(15271486669663284821)
XLA Ops:
  0.6 42.2 %fused.1 = (bf16[896,512]{1,0:T(8,128)(2,1)S(1)}, f32[128,512]{1,0:T(8,128)S(1)}, f32[28,16,128]{2,1,0:T(8,128)S(1)}) custom-call(s32[16,112]{1,0:T(8,128)} %bitcast.3, bf16[28,32,128]{2,1,0:T(8,128)(2,1)} %bitcast.2, f32[8,896]{1,0:T(8,128)} %log_hbm.1, bf16[896,512]{1,0:T(8,128)(2,1)} %q_hbm.1, bf16[896,512]{1,0:T(8,128)(2,1)} %g_hbm.1, ...), custom_call_target="tpu_custom_call" | custom-call | tf_op jit(solution)/shard_map/fused/pallas_call | solution.py:659
  42.8 1.1 %finish.1 = (bf16[896,512]{1,0:T(8,128)(2,1)}, f32[128,512]{1,0:T(8,128)}, f32[28,16,128]{2,1,0:T(8,128)}) custom-call(bf16[896,512]{1,0:T(8,128)(2,1)S(1)} %get-tuple-element.9.qg_ref, f32[128,512]{1,0:T(8,128)S(1)} %get-tuple-element.10.wg_ref, f32[28,16,128]{2,1,0:T(8,128)S(1)} %get-tuple-element.11.kvg_ref), custom_call_target="tpu_custom_call" | custom-call | tf_op jit(solution)/shard_map/finish/pallas_call | solution.py:630
